TPU v7x, 32 devices: a whole 2x2x4 slice. The times are simulated.
32 devices in a mesh: grp: 2 (over y), sp: 4 (over z), tp: 4 (over x, core).
Axes of the slice: x: 2, y: 2, z: 4, core: 2. Of those that a mesh axis runs over, the one named last changes fastest.
Arguments:
- tokens: bfloat16 [3072, 2048], P(('grp', 'sp')), parts along dimension 0, may hold values from -6 to 6
- norm_gain: float32 [2, 2048], replicated, may hold values from 0.1 to 1.9
- entry_weight: bfloat16 [2, 2048, 2048], P(None, 'sp', 'tp'), may hold values from -0.125 to 0.125
- mix_weight: bfloat16 [2, 4, 512, 512], P(None, 'tp'), may hold values from -0.25 to 0.25
- pool_gain: float32 [2, 2048], P(None, 'tp'), may hold values from 0.1 to 1.9
- back_weight: bfloat16 [2, 2048, 2048], P(None, 'tp', 'sp'), may hold values from -0.25 to 0.25
Outputs:
- result_tokens: bfloat16 [3072, 2048], P(('grp', 'sp')), parts along dimension 0
There are 2 independent parts, one for each index of `grp`. A program takes and returns all parts, laid end to end along the dimension named above; an argument that names none is the same for every part. Nothing has to cross between parts.
All inputs are finite; a program needn't handle non-finite values.
Results may differ from a plain program's by a relative error of at most 0.018.
Values may be sent and summed in bfloat16 or wider, within the bound.
A program may use at most 64 MiB of HBM per device.

v0:
```python
import jax
import jax.numpy as jnp
from jax import lax
from jax.sharding import PartitionSpec as P

GROUPS = 4
LAYERS = 2
EPSILON = 1e-05


def extended_2(value, sides, width):
    for axis, dim in sides:
        size, length = (lax.axis_size(axis), value.shape[dim])
        up = [(i, (i + 1) % size) for i in range(size - 1)]
        down = [(j, i) for i, j in up]
        last = lax.slice_in_dim(value, length - width, length, axis=dim)
        first = lax.slice_in_dim(value, 0, width, axis=dim)
        before = lax.ppermute(last, axis, up)
        after = lax.ppermute(first, axis, down)
        value = jnp.concatenate([before, value, after], axis=dim)
    return value


def window_mean(padded, positions, halves, total_length, reach):
    row_count = positions.shape[0]
    summed = jnp.zeros((row_count,) + padded.shape[1:], jnp.float32)
    for offset in range(-reach, reach):
        inside = ((offset >= -halves) & (offset < halves)).astype(jnp.float32)
        summed = (
            summed + padded[reach + offset : reach + offset + row_count] * inside[None, :, None]
        )
    lower = jnp.maximum(positions[:, None] - halves[None, :], 0)
    upper = jnp.minimum(positions[:, None] + halves[None, :], total_length)
    counted = (upper - lower).astype(jnp.float32)
    return summed / counted[:, :, None]


def normalize(state, gain):
    values = state.astype(jnp.float32)
    scaled = values * lax.rsqrt(jnp.mean(values * values, axis=-1, keepdims=True) + EPSILON)
    return (scaled * gain).astype(jnp.bfloat16)


def pool_groups(pooled_in, mix_layer, gain_layer, reach):
    row_count = pooled_in.shape[0]
    group_here = mix_layer.shape[0]
    width = mix_layer.shape[1]
    extended = extended_2(pooled_in, (("sp", 0),), reach)
    first_group = lax.axis_index("tp") * group_here
    halves = jnp.left_shift(jnp.int32(1), first_group + jnp.arange(group_here, dtype=jnp.int32))
    positions = lax.axis_index("sp") * row_count + jnp.arange(row_count, dtype=jnp.int32)
    total_length = lax.axis_size("sp") * row_count
    padded = extended.reshape(row_count + 2 * reach, group_here, width).astype(jnp.float32)
    means = window_mean(padded, positions, halves, total_length, reach)
    differ = (means - padded[reach : reach + row_count]).astype(jnp.bfloat16)
    mixed = jnp.einsum("tgc,gcd->tgd", differ, mix_layer, preferred_element_type=jnp.float32)
    return (mixed.reshape(row_count, group_here * width) * gain_layer).astype(jnp.bfloat16)


def per_device(tokens, norm_gain, entry_weight, mix_weight, pool_gain, back_weight):
    reach = 2 ** (GROUPS - 1)
    state = tokens
    entry_all, back_all = (
        lax.all_gather(entry_weight, "sp", axis=1, tiled=True),
        lax.all_gather(back_weight, "sp", axis=2, tiled=True),
    )
    for layer in range(LAYERS):
        normed = normalize(state, norm_gain[layer])
        pooled_in = jnp.dot(normed, entry_all[layer], preferred_element_type=jnp.float32).astype(
            jnp.bfloat16
        )
        back_local = back_all[layer]
        mixed = pool_groups(pooled_in, mix_weight[layer], pool_gain[layer], reach)
        update = jnp.dot(mixed, back_local, preferred_element_type=jnp.float32)
        summed = lax.psum(update.astype(jnp.bfloat16), "tp").astype(jnp.float32)
        state = (state.astype(jnp.float32) + summed).astype(jnp.bfloat16)
    return state


def solution(mesh):
    return jax.shard_map(
        per_device,
        mesh=mesh,
        in_specs=(
            P(("grp", "sp"), None),
            P(),
            P(None, "sp", "tp"),
            P(None, "tp", None, None),
            P(None, "tp"),
            P(None, "tp", "sp"),
        ),
        out_specs=P(("grp", "sp"), None),
        check_vma=False,
    )
```

profile of v0, /device:TPU:0, one launch (start us, length us, event | category | flops | bytes accessed | tf_op | source)
XLA Modules:
  0.0 298.0 jit_solution(13952838582287595426)
XLA Ops:
  6.5 0.0 copy-start
  6.5 0.0 copy-start.3
  6.5 0.0 copy-start.2
  6.5 0.0 all-gather.3.cloned.1.call-start
  6.5 0.7 all-gather.3.cloned.1.call-update
  7.3 0.0 all-gather.5.cloned.1.call-start
  7.3 0.7 all-gather.5.cloned.1.call-update
  8.0 0.0 all-reduce.3.cloned.1.call-start
  8.1 0.0 copy-done
  8.1 0.4 fusion
  8.5 0.0 copy-done.3
  8.5 0.0 copy-done.2
  8.5 83.9 %all-gather.3.cloned.1.call-done = bf16[2,2048,512]{2,1,0:T(8,128)(2,1)} async-done(((bf16[2,512,512]{2,1,0:T(8,128)(2,1)}), bf16[2,2048,512]{2,1,0:T(8,128)(2,1)}) %all-gather.3.cloned.1.call-update) | async-done | bytes 4194320 | tf_op jit(solution)/shard_map/all_gather | solution.py:64
  92.4 2.6 fusion.20
  95.0 1.3 collective-permute-start
  96.3 1.3 collective-permute-start.1
  97.8 0.0 collective-permute-done
  97.8 4.2 %collective-permute-done.1 = bf16[8,512]{1,0:T(8,128)(2,1)S(1)} collective-permute-done((bf16[8,512]{1,0:T(8,128)(2,1)S(1)}, bf16[8,512]{1,0:T(8,128)(2,1)S(1)}, u32[]{:S(2)}, u32[]{:S(2)}) %collective-permute-start.1) | collective-permute-done | bytes 8224 | tf_op jit(solution)/shard_map/ppermute | solution.py:19
  101.9 0.1 maximum_convert_fusion
  102.0 71.2 %all-gather.5.cloned.1.call-done = bf16[2,512,2048]{2,1,0:T(8,128)(2,1)} async-done(((bf16[2,512,512]{2,1,0:T(8,128)(2,1)}), bf16[2,512,2048]{2,1,0:T(8,128)(2,1)}) %all-gather.5.cloned.1.call-update) | async-done | bytes 4194320 | tf_op jit(solution)/shard_map/all_gather | solution.py:65
  173.2 5.3 %convolution_convert_fusion.1 = bf16[384,2048]{1,0:T(8,128)(2,1)} fusion(bf16[2,512,2048]{2,1,0:T(8,128)(2,1)} %all-gather.5.cloned.1.call-done, bf16[2,1,512,512]{3,2,1,0:T(8,128)(2,1)} %param.9, f32[512]{0:T(512)S(1)} %bitcast.87, f32[400,1,512]{2,0,1:T(8,128)S(1)} %maximum_convert_fusion, f32[384]{0:T(512)S(1)} %subtract_convert_fusion, f32[]{:T(128)S(6)} %mul.373, ...), kind=kOutput, calls=%fused_computation.15 | convolution fusion | flops 1014497280 | bytes 16781376 | tf_op jit(solution)/shard_map/dot_general | solution.py:74
  178.5 0.0 all-reduce.3.cloned.1.call-update
  178.5 0.0 all-reduce.5.cloned.1.call-start
  178.6 41.4 %all-reduce.3.cloned.1.call-done = bf16[384,2048]{1,0:T(8,128)(2,1)} async-done(((bf16[384,2048]{1,0:T(8,128)(2,1)}), bf16[384,2048]{1,0:T(8,128)(2,1)}) %all-reduce.3.cloned.1.call-update) | async-done | bytes 1572880 | tf_op jit(solution)/shard_map/psum | solution.py:75
  220.0 0.0 copy-start.1
  220.0 2.1 fusion.4
  222.1 0.0 copy-done.1
  222.1 2.6 fusion.23
  224.8 3.4 %collective-permute-start.2 = (bf16[8,512]{1,0:T(8,128)(2,1)S(1)}, bf16[8,512]{1,0:T(8,128)(2,1)S(1)}, u32[]{:S(2)}, u32[]{:S(2)}) collective-permute-start(bf16[8,512]{1,0:T(8,128)(2,1)S(1)} %get-tuple-element.5), channel_id=1, source_target_pairs={{0,4},{4,8},{8,12},{1,5},{5,9},{9,13},{2,6},{6,10},{10,14},{3,7},{... | collective-permute-start | bytes 24584 | tf_op jit(solution)/shard_map/ppermute | solution.py:18
  228.2 1.3 collective-permute-start.3
  229.5 0.0 collective-permute-done.2
  229.5 4.2 %collective-permute-done.3 = bf16[8,512]{1,0:T(8,128)(2,1)S(1)} collective-permute-done((bf16[8,512]{1,0:T(8,128)(2,1)S(1)}, bf16[8,512]{1,0:T(8,128)(2,1)S(1)}, u32[]{:S(2)}, u32[]{:S(2)}) %collective-permute-start.3) | collective-permute-done | bytes 8224 | tf_op jit(solution)/shard_map/ppermute | solution.py:19
  233.7 1.0 maximum_convert_fusion.1
  234.7 11.3 %convolution_convert_fusion = bf16[384,2048]{1,0:T(8,128)(2,1)} fusion(bf16[2,512,2048]{2,1,0:T(8,128)(2,1)} %all-gather.5.cloned.1.call-done, bf16[2,1,512,512]{3,2,1,0:T(8,128)(2,1)} %param.9, f32[512]{0:T(512)S(1)} %bitcast.86, f32[400,1,512]{2,0,1:T(8,128)} %maximum_convert_fusion.1, f32[384]{0:T(512)S(1)} %subtract_convert_fusion, f32[]{:T(128)S(6)} %mul.373, ...), kind=kOutput, calls=%fused_computation.14 | convolution fusion | flops 1014497280 | bytes 16780864 | tf_op jit(solution)/shard_map/dot_general | solution.py:74
  246.0 0.0 all-reduce.5.cloned.1.call-update
  246.0 42.1 %all-reduce.5.cloned.1.call-done = bf16[384,2048]{1,0:T(8,128)(2,1)} async-done(((bf16[384,2048]{1,0:T(8,128)(2,1)}), bf16[384,2048]{1,0:T(8,128)(2,1)}) %all-reduce.5.cloned.1.call-update) | async-done | bytes 1572880 | tf_op jit(solution)/shard_map/psum | solution.py:75
  288.2 3.4 %fusion.7 = bf16[384,2048]{1,0:T(8,128)(2,1)} fusion(bf16[384,2048]{1,0:T(8,128)(2,1)} %all-reduce.5.cloned.1.call-done, bf16[384,2048]{1,0:T(8,128)(2,1)S(1)} %copy-done.1, bf16[384,2048]{1,0:T(8,128)(2,1)S(1)} %copy-done), kind=kLoop, calls=%fused_computation.13 | loop fusion | flops 6291456 | bytes 6291456 | tf_op jit(solution)/shard_map/convert_element_type | solution.py:76
  (7 shorter events, 0.1 us)
Async XLA Ops:
  6.5 1.5 copy-start
  6.5 1.9 copy-start.3
  6.5 2.0 copy-start.2
  6.5 85.9 %all-gather.3.cloned.1.call-start = ((), (), s32[]{:S(2)}) async-start(), calls=%async_computation | async-start | bytes 5242880 | tf_op jit(solution)/shard_map/all_gather | solution.py:64
  7.3 166.0 %all-gather.5.cloned.1.call-start = ((), (), s32[]{:S(2)}) async-start(), calls=%async_computation.1 | async-start | bytes 5242880 | tf_op jit(solution)/shard_map/all_gather | solution.py:65
  8.0 212.0 %all-reduce.3.cloned.1.call-start = ((), (), s32[]{:S(2)}) async-start(), calls=%async_computation.2 | async-start | bytes 3145728 | tf_op jit(solution)/shard_map/psum | solution.py:75
  95.0 2.7 collective-permute-start
  96.3 5.6 %collective-permute-start.1 = (bf16[8,512]{1,0:T(8,128)(2,1)S(1)}, bf16[8,512]{1,0:T(8,128)(2,1)S(1)}, u32[]{:S(2)}, u32[]{:S(2)}) collective-permute-start(bf16[8,512]{1,0:T(8,128)(2,1)S(1)} %get-tuple-element.8), channel_id=1, source_target_pairs={{4,0},{8,4},{12,8},{5,1},{9,5},{13,9},{6,2},{10,6},{14,10},{7,3},{... | collective-permute-start | bytes 24584 | tf_op jit(solution)/shard_map/ppermute | solution.py:19
  178.5 109.6 %all-reduce.5.cloned.1.call-start = ((), (), s32[]{:S(2)}) async-start(), calls=%async_computation.3 | async-start | bytes 3145728 | tf_op jit(solution)/shard_map/psum | solution.py:75
  220.0 2.1 copy-start.1
  224.8 4.7 %collective-permute-start.2 = (bf16[8,512]{1,0:T(8,128)(2,1)S(1)}, bf16[8,512]{1,0:T(8,128)(2,1)S(1)}, u32[]{:S(2)}, u32[]{:S(2)}) collective-permute-start(bf16[8,512]{1,0:T(8,128)(2,1)S(1)} %get-tuple-element.5), channel_id=1, source_target_pairs={{0,4},{4,8},{8,12},{1,5},{5,9},{9,13},{2,6},{6,10},{10,14},{3,7},{... | collective-permute-start | bytes 24584 | tf_op jit(solution)/shard_map/ppermute | solution.py:18
  228.2 5.5 %collective-permute-start.3 = (bf16[8,512]{1,0:T(8,128)(2,1)S(1)}, bf16[8,512]{1,0:T(8,128)(2,1)S(1)}, u32[]{:S(2)}, u32[]{:S(2)}) collective-permute-start(bf16[8,512]{1,0:T(8,128)(2,1)S(1)} %get-tuple-element.6), channel_id=1, source_target_pairs={{4,0},{8,4},{12,8},{5,1},{9,5},{13,9},{6,2},{10,6},{14,10},{7,3},{... | collective-permute-start | bytes 24584 | tf_op jit(solution)/shard_map/ppermute | solution.py:19
Sparse Core Ops, SparseCore 0:
  8.9 83.4 all-gather.2
  94.0 79.2 all-gather.4
  178.6 41.3 all-reduce.2
  246.1 41.9 all-reduce.4
where the time goes:
time: 298 us
  waiting for transfers between devices  249 us (84%)
  matrix products  21.8 us (7%)
  between operations  13.4 us (4%)
  starting transfers between devices  7.37 us (2%)
  other arithmetic  6.97 us (2%)
    all_gather x1, waiting for transfers between devices, per_device(): lax.all_gather(entry_weight, 'sp', axis=1, tiled=True)  83.9 us
    psum x2, waiting for transfers between devices, per_device(): summed = lax.psum(update.astype(jnp.bfloat16), 'tp').astype(jnp.float32)  83.6 us
    all_gather x1, waiting for transfers between devices, per_device(): lax.all_gather(back_weight, 'sp', axis=2, tiled=True)  71.2 us
    dot_general x2, matrix products, per_device(): update = jnp.dot(mixed, back_local, preferred_element_type=jnp.float32)  16.5 us
    ppermute x2, waiting for transfers between devices, extended_2(): after = lax.ppermute(first, axis, down)  8.37 us
  transfers between devices with their start and end apart: 8, of which 6 were waited for; matrix products, arithmetic and copies ran while one was open for 1% of the time, Pallas kernels for 0%

commit v1 on v0

--- a/solution.py
+++ b/solution.py
@@ -62,7 +62,7 @@
     state = tokens
     entry_all, back_all = (
         lax.all_gather(entry_weight, "sp", axis=1, tiled=True),
-        lax.all_gather(back_weight, "sp", axis=2, tiled=True),
+        jnp.concatenate(jax.lax.all_gather(back_weight, "sp"), axis=2),
     )
     for layer in range(LAYERS):
         normed = normalize(state, norm_gain[layer])

time: 298 us -> 309 us (1.037)
  local copies, waits for them, and re-layouts: 0.04 us -> 14 us
  waiting for transfers between devices: 249 us -> 241 us
  starting transfers between devices: 7.37 us -> 11.8 us
    slice x0 -> x3, local copies, waits for them, and re-layouts: none -> 12.8 us  [per_device(): back_local = back_all[layer]]
    ppermute x2, waiting for transfers between devices: 8.37 us -> 0.01 us  [extended_2(): after = lax.ppermute(first, axis, down)]
    ppermute x2, starting transfers between devices: 4.67 us -> 9.09 us  [extended_2(): before = lax.ppermute(last, axis, up)]
  transfers between devices with their start and end apart: 8 -> 8, of which waited for: 6 -> 4; matrix products, arithmetic and copies ran while one was open for 1% -> 5% of each run, Pallas kernels for 0% -> 0%
where the time goes in v1:
time: 309 us
  waiting for transfers between devices  241 us (78%)
  matrix products  22.3 us (7%)
  local copies, waits for them, and re-layouts  14 us (5%)
  between operations  13.4 us (4%)
  starting transfers between devices  11.8 us (4%)
  other arithmetic  7.01 us (2%)
    psum x2, waiting for transfers between devices, per_device(): summed = lax.psum(update.astype(jnp.bfloat16), 'tp').astype(jnp.float32)  83.6 us
    all_gather x1, waiting for transfers between devices, per_device(): lax.all_gather(entry_weight, 'sp', axis=1, tiled=True)  83.2 us
    all_gather x1, waiting for transfers between devices, per_device(): jax.lax.all_gather(back_weight, 'sp')  72.3 us
    dot_general x2, matrix products, per_device(): update = jnp.dot(mixed, back_local, preferred_element_type=jnp.float32)  17.1 us
    slice x3, local copies, waits for them, and re-layouts, per_device(): back_local = back_all[layer]  12.8 us
    ppermute x2, starting transfers between devices, extended_2(): before = lax.ppermute(last, axis, up)  9.09 us
  transfers between devices with their start and end apart: 8, of which 4 were waited for; matrix products, arithmetic and copies ran while one was open for 5% of the time, Pallas kernels for 0%

profile of v1, /device:TPU:0, one launch (start us, length us, event | category | flops | bytes accessed | tf_op | source)
XLA Modules:
  0.0 309.0 jit_solution(2619314944814629742)
XLA Ops:
  6.5 0.0 copy-start
  6.5 0.0 copy-start.3
  6.5 0.0 copy-start.2
  6.5 0.0 all-gather.4.cloned.1.call-start
  6.5 0.7 all-gather.4.cloned.1.call-update
  7.3 0.0 all-gather.6.cloned.1.call-start
  7.3 0.7 all-gather.6.cloned.1.call-update
  8.0 0.0 all-reduce.3.cloned.1.call-start
  8.2 0.0 copy-done
  8.2 0.0 copy-start.4
  8.2 0.4 fusion
  8.6 0.0 copy-done.3
  8.6 0.5 fusion.87
  9.2 0.0 copy-done.2
  9.2 83.2 %all-gather.4.cloned.1.call-done = bf16[2,2048,512]{2,1,0:T(8,128)(2,1)} async-done(((bf16[2,512,512]{2,1,0:T(8,128)(2,1)}), bf16[2,2048,512]{2,1,0:T(8,128)(2,1)}) %all-gather.4.cloned.1.call-update) | async-done | bytes 4194320 | tf_op jit(solution)/shard_map/all_gather | solution.py:64
  92.4 2.6 fusion.20
  95.0 1.3 collective-permute-start.1
  96.3 4.5 %collective-permute-start = (bf16[8,512]{1,0:T(8,128)(2,1)S(1)}, bf16[8,512]{1,0:T(8,128)(2,1)S(1)}, u32[]{:S(2)}, u32[]{:S(2)}) collective-permute-start(bf16[8,512]{1,0:T(8,128)(2,1)S(1)} %get-tuple-element.9), channel_id=1, source_target_pairs={{0,4},{4,8},{8,12},{1,5},{5,9},{9,13},{2,6},{6,10},{10,14},{3,7},{... | collective-permute-start | bytes 24584 | tf_op jit(solution)/shard_map/ppermute | solution.py:18
  100.9 72.3 %all-gather.6.cloned.1.call-done = bf16[8,512,512]{2,1,0:T(8,128)(2,1)} async-done(((bf16[2,512,512]{2,1,0:T(8,128)(2,1)}), bf16[8,512,512]{2,1,0:T(8,128)(2,1)}) %all-gather.6.cloned.1.call-update) | async-done | bytes 4194320 | tf_op jit(solution)/shard_map/all_gather | solution.py:65
  173.2 4.5 %fusion.83 = (bf16[1,512,4,512]{3,1,0,2:T(8,128)(2,1)}, bf16[1,512,4,512]{3,1,0,2:T(8,128)(2,1)}) fusion(bf16[2,512,4,512]{3,1,0,2:T(8,128)(2,1)} %bitcast.79), kind=kLoop, calls=%fused_computation.113 | loop fusion | bytes 8388608 | tf_op jit(solution)/shard_map/slice | solution.py:72
  177.7 4.2 %copy.9 = bf16[1,512,4,512]{1,3,2,0:T(8,128)(2,1)} copy(bf16[1,512,4,512]{3,1,0,2:T(8,128)(2,1)} %get-tuple-element.5) | data formatting | bytes 4194304 | tf_op jit(solution)/shard_map/slice | solution.py:72
  181.9 0.0 collective-permute-done.1
  181.9 0.0 collective-permute-done
  181.9 0.1 maximum_convert_fusion
  182.0 0.0 copy-done.4
  182.0 5.3 %convolution_convert_fusion.1 = bf16[384,2048]{1,0:T(8,128)(2,1)} fusion(bf16[512,2048]{0,1:T(8,128)(2,1)} %bitcast.81, bf16[2,1,512,512]{3,2,1,0:T(8,128)(2,1)} %param.9, f32[512]{0:T(512)S(1)} %bitcast.91, f32[400,1,512]{2,0,1:T(8,128)S(1)} %maximum_convert_fusion, f32[384]{0:T(512)S(1)} %subtract_convert_fusion, f32[]{:T(128)S(6)} %mul.373, ...), kind=kOutput, calls=%fused_computation.15 | convolution fusion | flops 1014497280 | bytes 16781376 | tf_op jit(solution)/shard_map/dot_general | solution.py:74
  187.3 0.0 all-reduce.3.cloned.1.call-update
  187.3 0.0 all-reduce.5.cloned.1.call-start
  187.3 41.5 %all-reduce.3.cloned.1.call-done = bf16[384,2048]{1,0:T(8,128)(2,1)} async-done(((bf16[384,2048]{1,0:T(8,128)(2,1)}), bf16[384,2048]{1,0:T(8,128)(2,1)}) %all-reduce.3.cloned.1.call-update) | async-done | bytes 1572880 | tf_op jit(solution)/shard_map/psum | solution.py:75
  228.8 0.0 copy-start.1
  228.8 2.1 fusion.4
  230.9 0.0 copy-done.1
  230.9 2.6 fusion.23
  233.6 0.6 fusion.84
  234.2 1.3 collective-permute-start.3
  235.4 4.5 %collective-permute-start.2 = (bf16[8,512]{1,0:T(8,128)(2,1)}, bf16[8,512]{1,0:T(8,128)(2,1)S(1)}, u32[]{:S(2)}, u32[]{:S(2)}) collective-permute-start(bf16[8,512]{1,0:T(8,128)(2,1)} %get-tuple-element.7), channel_id=1, source_target_pairs={{0,4},{4,8},{8,12},{1,5},{5,9},{9,13},{2,6},{6,10},{10,14},{3,7},{... | collective-permute-start | bytes 24584 | tf_op jit(solution)/shard_map/ppermute | solution.py:18
  240.0 4.1 %copy.10 = bf16[1,512,4,512]{1,3,2,0:T(8,128)(2,1)} copy(bf16[1,512,4,512]{3,1,0,2:T(8,128)(2,1)} %get-tuple-element.6) | data formatting | bytes 4194304 | tf_op jit(solution)/shard_map/slice | solution.py:72
  244.1 0.0 collective-permute-done.3
  244.1 0.0 collective-permute-done.2
  244.1 1.0 maximum_convert_fusion.1
  245.2 11.8 %convolution_convert_fusion = bf16[384,2048]{1,0:T(8,128)(2,1)} fusion(bf16[512,2048]{0,1:T(8,128)(2,1)} %bitcast.80, bf16[2,1,512,512]{3,2,1,0:T(8,128)(2,1)} %param.9, f32[512]{0:T(512)} %bitcast.90, f32[400,1,512]{2,0,1:T(8,128)} %maximum_convert_fusion.1, f32[384]{0:T(512)} %copy-done.4, f32[]{:T(128)S(6)} %mul.373, f32[]{:T(128)S(6)} %mul.370, ...), kind=kOutput, calls=%fused_computation.14 | convolution fusion | flops 1014497280 | bytes 16781376 | tf_op jit(solution)/shard_map/dot_general | solution.py:74
  257.0 0.0 all-reduce.5.cloned.1.call-update
  257.0 42.1 %all-reduce.5.cloned.1.call-done = bf16[384,2048]{1,0:T(8,128)(2,1)} async-done(((bf16[384,2048]{1,0:T(8,128)(2,1)}), bf16[384,2048]{1,0:T(8,128)(2,1)}) %all-reduce.5.cloned.1.call-update) | async-done | bytes 1572880 | tf_op jit(solution)/shard_map/psum | solution.py:75
  299.1 3.4 %fusion.7 = bf16[384,2048]{1,0:T(8,128)(2,1)} fusion(bf16[384,2048]{1,0:T(8,128)(2,1)} %all-reduce.5.cloned.1.call-done, bf16[384,2048]{1,0:T(8,128)(2,1)S(1)} %copy-done.1, bf16[384,2048]{1,0:T(8,128)(2,1)S(1)} %copy-done), kind=kLoop, calls=%fused_computation.13 | loop fusion | flops 6291456 | bytes 6291456 | tf_op jit(solution)/shard_map/convert_element_type | solution.py:76
  (5 shorter events, 0.0 us)
Async XLA Ops:
  6.5 1.7 copy-start
  6.5 2.1 copy-start.3
  6.5 2.6 copy-start.2
  6.5 85.9 %all-gather.4.cloned.1.call-start = ((), (), s32[]{:S(2)}) async-start(), calls=%async_computation | async-start | bytes 5242880 | tf_op jit(solution)/shard_map/all_gather | solution.py:64
  7.3 166.0 %all-gather.6.cloned.1.call-start = ((), (), s32[]{:S(2)}) async-start(), calls=%async_computation.3 | async-start | bytes 5242880 | tf_op jit(solution)/shard_map/all_gather | solution.py:65
  8.0 220.8 %all-reduce.3.cloned.1.call-start = ((), (), s32[]{:S(2)}) async-start(), calls=%async_computation.1 | async-start | bytes 3145728 | tf_op jit(solution)/shard_map/psum | solution.py:75
  8.2 173.8 %copy-start.4 = (f32[384]{0:T(512)}, f32[384]{0:T(512)S(1)}, u32[]{:S(2)}) copy-start(f32[384]{0:T(512)S(1)} %subtract_convert_fusion) | copy-start | bytes 4612
  95.0 86.8 %collective-permute-start.1 = (bf16[8,512]{1,0:T(8,128)(2,1)S(1)}, bf16[8,512]{1,0:T(8,128)(2,1)S(1)}, u32[]{:S(2)}, u32[]{:S(2)}) collective-permute-start(bf16[8,512]{1,0:T(8,128)(2,1)S(1)} %get-tuple-element.10), channel_id=1, source_target_pairs={{4,0},{8,4},{12,8},{5,1},{9,5},{13,9},{6,2},{10,6},{14,10},{7,3},{... | collective-permute-start | bytes 24584 | tf_op jit(solution)/shard_map/ppermute | solution.py:19
  96.3 85.5 %collective-permute-start = (bf16[8,512]{1,0:T(8,128)(2,1)S(1)}, bf16[8,512]{1,0:T(8,128)(2,1)S(1)}, u32[]{:S(2)}, u32[]{:S(2)}) collective-permute-start(bf16[8,512]{1,0:T(8,128)(2,1)S(1)} %get-tuple-element.9), channel_id=1, source_target_pairs={{0,4},{4,8},{8,12},{1,5},{5,9},{9,13},{2,6},{6,10},{10,14},{3,7},{... | collective-permute-start | bytes 24584 | tf_op jit(solution)/shard_map/ppermute | solution.py:18
  187.3 111.8 %all-reduce.5.cloned.1.call-start = ((), (), s32[]{:S(2)}) async-start(), calls=%async_computation.2 | async-start | bytes 3145728 | tf_op jit(solution)/shard_map/psum | solution.py:75
  228.8 2.1 copy-start.1
  234.2 10.0 %collective-permute-start.3 = (bf16[8,512]{1,0:T(8,128)(2,1)}, bf16[8,512]{1,0:T(8,128)(2,1)S(1)}, u32[]{:S(2)}, u32[]{:S(2)}) collective-permute-start(bf16[8,512]{1,0:T(8,128)(2,1)} %get-tuple-element.8), channel_id=1, source_target_pairs={{4,0},{8,4},{12,8},{5,1},{9,5},{13,9},{6,2},{10,6},{14,10},{7,3},{... | collective-permute-start | bytes 24584 | tf_op jit(solution)/shard_map/ppermute | solution.py:19
  235.4 8.7 %collective-permute-start.2 = (bf16[8,512]{1,0:T(8,128)(2,1)}, bf16[8,512]{1,0:T(8,128)(2,1)S(1)}, u32[]{:S(2)}, u32[]{:S(2)}) collective-permute-start(bf16[8,512]{1,0:T(8,128)(2,1)} %get-tuple-element.7), channel_id=1, source_target_pairs={{0,4},{4,8},{8,12},{1,5},{5,9},{9,13},{2,6},{6,10},{10,14},{3,7},{... | collective-permute-start | bytes 24584 | tf_op jit(solution)/shard_map/ppermute | solution.py:18
Sparse Core Ops, SparseCore 0:
  8.9 83.4 all-gather.3
  94.0 79.2 all-gather.5
  187.4 41.3 all-reduce.2
  257.1 41.9 all-reduce.4
